TPU v7x, 32 devices: a whole 2x2x4 slice. The times are simulated.
32 devices in a mesh: sp: 8 (over z, x), tp: 4 (over y, core).
Axes of the slice: x: 2, y: 2, z: 4, core: 2. Of those that a mesh axis runs over, the one named last changes fastest.
Arguments:
- tokens: bfloat16 [6144, 2048], P('sp', 'tp'), may hold values from -23 to 23, as said below
- norm_gain: float32 [2048], replicated, may hold values from 0.8 to 8, as said below
- window_query: bfloat16 [2048, 1024], P(None, 'tp'), may hold values from -0.125 to 0.125
- window_key: bfloat16 [2048, 512], P(None, 'tp'), may hold values from -0.125 to 0.125
- window_value: bfloat16 [2048, 512], P(None, 'tp'), may hold values from -0.125 to 0.125
- sink_logit: float32 [16], P('tp'), may hold values from 2 to 6
- down_query: bfloat16 [2048, 768], replicated, may hold values from -0.125 to 0.125
- down_latent: bfloat16 [2048, 512], replicated, may hold values from -0.125 to 0.125
- rotary_proj: bfloat16 [2048, 32], replicated, may hold values from -0.125 to 0.125
- query_gain: float32 [768], replicated, may hold values from 0.8 to 8, as said below
- latent_gain: float32 [512], replicated, may hold values from 0.8 to 8, as said below
- up_query: bfloat16 [768, 1536], P(None, 'tp'), may hold values from -0.21875 to 0.21875
- up_key: bfloat16 [512, 1024], P(None, 'tp'), may hold values from -0.25 to 0.25
- up_value: bfloat16 [512, 1024], P(None, 'tp'), may hold values from -0.25 to 0.25
- window_out: bfloat16 [1024, 2048], P('tp'), may hold values from -0.125 to 0.125
- latent_out: bfloat16 [1024, 2048], P('tp'), may hold values from -0.125 to 0.125
Outputs:
- mixed: bfloat16 [6144, 2048], P(('sp', 'tp'))
Inputs may be any that keep to these rules, and one draw needn't show every extreme that they name: `tokens`: real-valued; the channels carry scales that vary smoothly by a factor of up to twenty across the width. `norm_gain`: positive. `query_gain`: positive. `latent_gain`: positive.
All inputs are finite; a program needn't handle non-finite values.
Results may differ from a plain program's by a relative error of at most 0.04.
The roundings to bfloat16 on the way count: a program that leaves them out, or rounds other values in their place, can miss the bound.
Values may be sent and summed in bfloat16 or wider, within the bound.
No kernel may reach another device: no remote copies, remote signals or barrier semaphores. Data moves between devices by JAX's collectives and lax.ppermute only.
A program may use at most 128 MiB of HBM per device.

v0:
```python
import jax
import jax.numpy as jnp
from jax import lax
from jax.sharding import PartitionSpec as P

D = 2048
A_HEADS = 16
HD = 64
NOPE = 64
ROPE = 32
VD = 64
WINDOW = 128
QBLOCK = 256


EPS = 1e-06
THETA = 10000.0
key_span = 1024


def with_halo(x, sides, width):
    for axis, dim in sides:
        size, length = (lax.axis_size(axis), x.shape[dim])
        up = [(i, (i + 1) % size) for i in range(size - 1)]
        down = [(j, i) for i, j in up]
        last = lax.slice_in_dim(x, length - width, length, axis=dim)
        initial = lax.slice_in_dim(x, 0, width, axis=dim)
        before = lax.ppermute(last, axis, up)
        after = lax.ppermute(initial, axis, down)
        x = jnp.concatenate([before, x, after], axis=dim)
    return x


def rotate(vector, positions):
    half_len = vector.shape[-1] // 2
    inverse = THETA ** (-jnp.arange(half_len, dtype=jnp.float32) / half_len)
    angles = positions.astype(jnp.float32)[:, None] * inverse[None, :]
    new_shape = (angles.shape[0],) + (1,) * (vector.ndim - 2) + (half_len,)
    cosine = jnp.cos(angles).reshape(new_shape)
    sine_part = jnp.sin(angles).reshape(new_shape)
    front_half = vector[..., :half_len].astype(jnp.float32)
    second = vector[..., half_len:].astype(jnp.float32)
    return jnp.concatenate(
        [front_half * cosine - second * sine_part, second * cosine + front_half * sine_part],
        axis=-1,
    )


def norm_rows(values, gain_vec):
    as_float = values.astype(jnp.float32)
    return (
        as_float * lax.rsqrt(jnp.mean(as_float * as_float, axis=1, keepdims=True) + EPS) * gain_vec
    ).astype(jnp.bfloat16)


def attend(running, q_nope, q_rot, key_rows, value_rows, rot_keys, lat_scale):
    prior_max, denom_sum, weighted = running
    scores = (
        jnp.einsum("qhd,khd->hqk", q_nope, key_rows, preferred_element_type=jnp.float32)
        + jnp.einsum("qhr,kr->hqk", q_rot, rot_keys, preferred_element_type=jnp.float32)
    ) * lat_scale
    row_max = jnp.maximum(prior_max, jnp.max(scores, axis=2))
    rescale = jnp.exp(prior_max - row_max)
    weights = jnp.exp(scores - row_max[:, :, None])
    denom_sum = denom_sum * rescale + jnp.sum(weights, axis=2)
    weighted = weighted * rescale.T[:, :, None] + jnp.einsum(
        "hqk,khd->qhd", weights.astype(jnp.bfloat16), value_rows, preferred_element_type=jnp.float32
    )
    return (row_max, denom_sum, weighted)


def in_blocks(running, arrays, block_fn):
    key_count = arrays[0].shape[0]
    blocked = tuple(
        (member.reshape((key_count // key_span, key_span) + member.shape[1:]) for member in arrays)
    )

    def scan_step(state_now, key_block):
        return (block_fn(state_now, key_block), None)

    running, unused = lax.scan(scan_step, running, blocked)
    return running


def per_device(
    tokens,
    norm_gain,
    window_query,
    window_key,
    window_value,
    sink_logit,
    down_query,
    down_latent,
    rotary_proj,
    query_gain,
    latent_gain,
    up_query,
    up_key,
    up_value,
    window_out,
    latent_out,
):
    row_count = tokens.shape[0]
    projections = (window_query, window_key, window_value, down_query, down_latent, rotary_proj)
    start_carry = (jnp.zeros((row_count,), jnp.float32),) + tuple(
        (jnp.zeros((row_count, weight.shape[1]), jnp.float32) for weight in projections)
    )
    as_float = lax.all_gather(tokens, "tp", axis=1, tiled=True).astype(jnp.float32)
    scaled = (as_float * norm_gain[None, :]).astype(jnp.bfloat16)
    updated = [jnp.sum(as_float * as_float, axis=1)]
    for total_now, weight in zip(start_carry[1:], projections):
        updated.append(jnp.dot(scaled, weight, preferred_element_type=jnp.float32))
    folded = tuple(updated)
    row_scale = lax.rsqrt(folded[0] / D + EPS)[:, None]
    q_window, k_window, v_window, latent_q, latent_kv, rotary_rows = [
        (member * row_scale).astype(jnp.bfloat16) for member in folded[1:]
    ]
    seq_index = lax.axis_index("sp")
    positions = seq_index * row_count + jnp.arange(row_count, dtype=jnp.int32)
    heads_dev = window_query.shape[1] // HD
    kv_dev = window_key.shape[1] // HD
    group = heads_dev // kv_dev
    stacked = jnp.concatenate([k_window, v_window], axis=1)
    padded = with_halo(stacked, (("sp", 0),), WINDOW)
    span_len = QBLOCK + 2 * WINDOW
    block_count = row_count // QBLOCK
    spans = jnp.stack(
        [
            padded[block_num * QBLOCK : block_num * QBLOCK + span_len]
            for block_num in range(block_count)
        ]
    )
    key_part = spans[..., : kv_dev * HD].reshape(block_count, span_len, kv_dev, HD)
    value_part = spans[..., kv_dev * HD :].reshape(block_count, span_len, kv_dev, HD)
    queries = q_window.reshape(block_count, QBLOCK, kv_dev, group, HD)
    scores = jnp.einsum(
        "nqhgd,nkhd->nhgqk", queries, key_part, preferred_element_type=jnp.float32
    ) * HD ** (-0.5)
    distance = jnp.arange(QBLOCK)[:, None] + WINDOW - jnp.arange(span_len)[None, :]
    head_ids = lax.axis_index("tp") * heads_dev + jnp.arange(heads_dev, dtype=jnp.int32)
    slopes = jnp.exp2(-8.0 * (head_ids.astype(jnp.float32) + 1.0) / A_HEADS).reshape(kv_dev, group)
    scores = scores - slopes[None, :, :, None, None] * jnp.abs(distance).astype(jnp.float32)
    key_pos = (
        seq_index * row_count
        + (jnp.arange(block_count, dtype=jnp.int32) * QBLOCK)[:, None]
        + jnp.arange(span_len, dtype=jnp.int32)[None, :]
        - WINDOW
    )
    seq_len = row_count * lax.axis_size("sp")
    valid = (jnp.abs(distance) <= WINDOW)[None] & ((key_pos >= 0) & (key_pos < seq_len))[:, None, :]
    scores = jnp.where(valid[:, None, None], scores, -jnp.inf)
    sinks = sink_logit.reshape(kv_dev, group)[None, :, :, None, None]
    row_max = jnp.maximum(jnp.max(scores, axis=4, keepdims=True), sinks)
    weights = jnp.exp(scores - row_max)
    weights = weights / (jnp.sum(weights, axis=4, keepdims=True) + jnp.exp(sinks - row_max))
    out_window = (
        jnp.einsum(
            "nhgqk,nkhd->nqhgd",
            weights.astype(jnp.bfloat16),
            value_part,
            preferred_element_type=jnp.float32,
        )
        .astype(jnp.bfloat16)
        .reshape(row_count, heads_dev * HD)
    )
    latent_heads = up_query.shape[1] // (NOPE + ROPE)
    q_latent = jnp.dot(
        norm_rows(latent_q, query_gain), up_query, preferred_element_type=jnp.float32
    ).astype(jnp.bfloat16)
    q_latent = q_latent.reshape(row_count, latent_heads, NOPE + ROPE)
    q_nope = q_latent[..., :NOPE]
    q_rot = rotate(q_latent[..., NOPE:], positions).astype(jnp.bfloat16)
    k_rot = rotate(rotary_rows, positions).astype(jnp.bfloat16)
    normed_kv = norm_rows(latent_kv, latent_gain)
    lat_scale = (NOPE + ROPE) ** (-0.5)
    start_state = (
        jnp.full((latent_heads, row_count), -1e30, jnp.float32),
        jnp.zeros((latent_heads, row_count), jnp.float32),
        jnp.zeros((row_count, latent_heads, VD), jnp.float32),
    )
    key_rows = jnp.dot(normed_kv, up_key, preferred_element_type=jnp.float32).astype(jnp.bfloat16)
    value_rows = jnp.dot(normed_kv, up_value, preferred_element_type=jnp.float32).astype(
        jnp.bfloat16
    )
    paired = jnp.concatenate([key_rows, value_rows], axis=1)

    def split_block(running, key_block):
        pair_part, rot_part = key_block
        key_count = pair_part.shape[0]
        return attend(
            running,
            q_nope,
            q_rot,
            pair_part[:, : latent_heads * NOPE].reshape(key_count, latent_heads, NOPE),
            pair_part[:, latent_heads * NOPE :].reshape(key_count, latent_heads, VD),
            rot_part,
            lat_scale,
        )

    final_state = in_blocks(
        start_state,
        (
            lax.all_gather(paired, "sp", axis=0, tiled=True),
            lax.all_gather(k_rot, "sp", axis=0, tiled=True),
        ),
        split_block,
    )
    out_latent = (
        (final_state[2] / final_state[1].T[:, :, None])
        .astype(jnp.bfloat16)
        .reshape(row_count, latent_heads * VD)
    )
    return lax.psum_scatter(
        (
            jnp.dot(out_window, window_out, preferred_element_type=jnp.float32)
            + jnp.dot(out_latent, latent_out, preferred_element_type=jnp.float32)
        ).astype(jnp.bfloat16),
        "tp",
        scatter_dimension=0,
        tiled=True,
    )


def solution(mesh):
    placed = (
        P("sp", "tp"),
        P(),
        P(None, "tp"),
        P(None, "tp"),
        P(None, "tp"),
        P("tp"),
        P(),
        P(),
        P(),
        P(),
        P(),
        P(None, "tp"),
        P(None, "tp"),
        P(None, "tp"),
        P("tp", None),
        P("tp", None),
    )
    return jax.shard_map(
        per_device, mesh=mesh, in_specs=placed, out_specs=P(("sp", "tp"), None), check_vma=False
    )
```

profile of v0, /device:TPU:0, one launch (start us, length us, event | category | flops | bytes accessed | tf_op | source)
XLA Modules:
  0.0 329.1 jit_solution(16561795479787083009)
XLA Ops:
  7.3 32.9 %all-gather.3.cloned.1.call-done = bf16[768,2048]{1,0:T(8,128)(2,1)} async-done(((bf16[768,512]{1,0:T(8,128)(2,1)}), bf16[768,2048]{1,0:T(8,128)(2,1)}) %all-gather.3.cloned.1.call-update) | async-done | bytes 3145744 | tf_op jit(solution)/shard_map/all_gather | solution.py:108
  40.2 2.7 fusion.18
  43.0 3.5 %fusion.26 = (f32[768]{0:T(1024)S(1)}, bf16[768,512]{0,1:T(8,128)(2,1)S(1)}) fusion(f32[768]{0:T(1024)S(1)} %add_rsqrt_fusion.2, bf16[2048,512]{1,0:T(8,128)(2,1)} %param.25, bf16[768,2048]{1,0:T(8,128)(2,1)S(1)} %copy-done.6, f32[2048]{0:T(1024)S(1)} %copy-done.25), kind=kOutput, calls=%fused_computation.39 | convolution fusion | flops 1617296640 | bytes 6043648 | tf_op jit(solution)/shard_map/dot_general | solution.py:112
  54.9 4.0 %collective-permute-start = (bf16[128,256]{0,1:T(8,128)(2,1)}, bf16[128,256]{0,1:T(8,128)(2,1)}, u32[]{:S(2)}, u32[]{:S(2)}) collective-permute-start(bf16[128,256]{0,1:T(8,128)(2,1)} %get-tuple-element.122), channel_id=1, source_target_pairs={{0,4},{4,8},{8,12},{12,16},{16,20},{20,24},{24,28},{1,5},{5,9},{9,... | collective-permute-start | bytes 196616 | tf_op jit(solution)/shard_map/ppermute | solution.py:28
  62.2 34.6 %all_gather.11 = bf16[6144,32]{0,1:T(8,128)(2,1)S(1)} all-gather(bf16[768,32]{0,1:T(8,128)(2,1)S(1)} %pad_maximum_fusion.9), channel_id=1, replica_groups=mesh['sp'=8,'tp'=4] {'sp'}, dimensions={0}, use_global_device_ids=true | all-gather | bytes 442368 | tf_op jit(solution)/shard_map/all_gather | solution.py:204
  99.3 2.8 reshape.240
  102.1 4.7 %fusion.23 = (f32[768]{0:T(1024)S(1)}, bf16[768,768]{0,1:T(8,128)(2,1)S(1)}) fusion(f32[768]{0:T(1024)} %copy-done.16, bf16[2048,768]{1,0:T(8,128)(2,1)S(1)} %copy-done, bf16[768,2048]{1,0:T(8,128)(2,1)} %all-gather.3.cloned.1.call-done, f32[2048]{0:T(1024)} %param.19), kind=kOutput, calls=%fused_computation.33 | convolution fusion | flops 2423586048 | bytes 7485440 | tf_op jit(solution)/shard_map/dot_general | solution.py:112
  113.2 2.0 fusion.42
  115.7 3.6 %fusion.91 = f32[768,2048]{1,0:T(8,128)} fusion(bf16[768,256]{0,1:T(8,128)(2,1)S(1)} %bitcast.110, bf16[256,2048]{1,0:T(8,128)(2,1)S(1)} %copy-done.8), kind=kOutput, calls=%fused_computation.124 | convolution fusion | flops 805306368 | bytes 7733248 | tf_op jit(solution)/shard_map/dot_general | solution.py:215
  119.3 32.7 %all-gather.5.cloned.1.call-done = bf16[6144,512]{0,1:T(8,128)(2,1)} async-done(((bf16[768,512]{0,1:T(8,128)(2,1)}), bf16[6144,512]{0,1:T(8,128)(2,1)}) %all-gather.5.cloned.1.call-update) | async-done | bytes 6291472 | tf_op jit(solution)/shard_map/all_gather | solution.py:203
  152.0 8.7 %copy.27 = bf16[6144,512]{1,0:T(8,128)(2,1)} copy(bf16[6144,512]{0,1:T(8,128)(2,1)} %all-gather.5.cloned.1.call-done) | data formatting | bytes 12582912 | tf_op jit(solution)/shard_map/all_gather | solution.py:203
  160.7 118.2 %while.15 = (s32[]{:T(128)}, f32[4,768]{1,0:T(4,128)S(1)}, f32[4,768]{1,0:T(4,128)S(1)}, f32[768,4,64]{0,2,1:T(8,128)}, bf16[6,1024,512]{2,1,0:T(8,128)(2,1)}, /...) while((s32[]{:T(128)}, f32[4,768]{1,0:T(4,128)S(1)}, ...), condition=%wide.region_8.9_spmd.clone, body=%wide.region_5.8_spmd.clone.sunk | while | flops 1029261312 | bytes 78971056 | solution.py:81
  162.6 6.4 %fusion.129 = f32[4,1024,768]{2,1,0:T(8,128)} fusion(bf16[1024,4,64]{0,2,1:T(8,128)(2,1)S(1)} %bitcast.107, bf16[768,4,64]{0,2,1:T(8,128)(2,1)S(1)} %get-tuple-element.222), kind=kOutput, calls=%fused_computation.123.clone.1 | convolution fusion | flops 402653184 | bytes 13500416 | tf_op jit(solution)/shard_map/while/body/eval_jaxpr/qhd,khd->hqk/dot_general | solution.py:59
  169.0 6.5 %fusion.130 = (f32[4,768]{1,0:T(4,128)S(1)}, f32[4,768,1024]{1,2,0:T(8,128)S(1)}) fusion(bf16[768,4,32]{0,2,1:T(8,128)(2,1)S(1)} %get-tuple-element.224, bf16[6,1024,32]{1,2,0:T(8,128)(2,1)} %get-tuple-element.223, s32[]{:T(128)S(6)} %copy.51, f32[4,1024,768]{2,1,0:T(8,128)} %fusion.129), kind=kOutput, calls=%fused_computation.121.clone.1 | convolution fusion | flops 210760704 | bytes 25440260 | tf_op jit(solution)/shard_map/while/body/eval_jaxpr/qhr,kr->hqk/dot_general | solution.py:60
  177.1 2.3 fusion.134
  182.3 6.4 %fusion.129 = f32[4,1024,768]{2,1,0:T(8,128)} fusion(bf16[1024,4,64]{0,2,1:T(8,128)(2,1)S(1)} %bitcast.107, bf16[768,4,64]{0,2,1:T(8,128)(2,1)S(1)} %get-tuple-element.222), kind=kOutput, calls=%fused_computation.123.clone.1 | convolution fusion | flops 402653184 | bytes 13500416 | tf_op jit(solution)/shard_map/while/body/eval_jaxpr/qhd,khd->hqk/dot_general | solution.py:59
  188.7 6.5 %fusion.130 = (f32[4,768]{1,0:T(4,128)S(1)}, f32[4,768,1024]{1,2,0:T(8,128)S(1)}) fusion(bf16[768,4,32]{0,2,1:T(8,128)(2,1)S(1)} %get-tuple-element.224, bf16[6,1024,32]{1,2,0:T(8,128)(2,1)} %get-tuple-element.223, s32[]{:T(128)S(6)} %copy.51, f32[4,1024,768]{2,1,0:T(8,128)} %fusion.129), kind=kOutput, calls=%fused_computation.121.clone.1 | convolution fusion | flops 210760704 | bytes 25440260 | tf_op jit(solution)/shard_map/while/body/eval_jaxpr/qhr,kr->hqk/dot_general | solution.py:60
  196.8 2.3 fusion.134
  202.0 6.3 %fusion.129 = f32[4,1024,768]{2,1,0:T(8,128)} fusion(bf16[1024,4,64]{0,2,1:T(8,128)(2,1)S(1)} %bitcast.107, bf16[768,4,64]{0,2,1:T(8,128)(2,1)S(1)} %get-tuple-element.222), kind=kOutput, calls=%fused_computation.123.clone.1 | convolution fusion | flops 402653184 | bytes 13500416 | tf_op jit(solution)/shard_map/while/body/eval_jaxpr/qhd,khd->hqk/dot_general | solution.py:59
  208.4 6.5 %fusion.130 = (f32[4,768]{1,0:T(4,128)S(1)}, f32[4,768,1024]{1,2,0:T(8,128)S(1)}) fusion(bf16[768,4,32]{0,2,1:T(8,128)(2,1)S(1)} %get-tuple-element.224, bf16[6,1024,32]{1,2,0:T(8,128)(2,1)} %get-tuple-element.223, s32[]{:T(128)S(6)} %copy.51, f32[4,1024,768]{2,1,0:T(8,128)} %fusion.129), kind=kOutput, calls=%fused_computation.121.clone.1 | convolution fusion | flops 210760704 | bytes 25440260 | tf_op jit(solution)/shard_map/while/body/eval_jaxpr/qhr,kr->hqk/dot_general | solution.py:60
  216.5 2.3 fusion.134
  221.7 6.3 %fusion.129 = f32[4,1024,768]{2,1,0:T(8,128)} fusion(bf16[1024,4,64]{0,2,1:T(8,128)(2,1)S(1)} %bitcast.107, bf16[768,4,64]{0,2,1:T(8,128)(2,1)S(1)} %get-tuple-element.222), kind=kOutput, calls=%fused_computation.123.clone.1 | convolution fusion | flops 402653184 | bytes 13500416 | tf_op jit(solution)/shard_map/while/body/eval_jaxpr/qhd,khd->hqk/dot_general | solution.py:59
  228.1 6.4 %fusion.130 = (f32[4,768]{1,0:T(4,128)S(1)}, f32[4,768,1024]{1,2,0:T(8,128)S(1)}) fusion(bf16[768,4,32]{0,2,1:T(8,128)(2,1)S(1)} %get-tuple-element.224, bf16[6,1024,32]{1,2,0:T(8,128)(2,1)} %get-tuple-element.223, s32[]{:T(128)S(6)} %copy.51, f32[4,1024,768]{2,1,0:T(8,128)} %fusion.129), kind=kOutput, calls=%fused_computation.121.clone.1 | convolution fusion | flops 210760704 | bytes 25440260 | tf_op jit(solution)/shard_map/while/body/eval_jaxpr/qhr,kr->hqk/dot_general | solution.py:60
  236.2 2.3 fusion.134
  241.4 6.3 %fusion.129 = f32[4,1024,768]{2,1,0:T(8,128)} fusion(bf16[1024,4,64]{0,2,1:T(8,128)(2,1)S(1)} %bitcast.107, bf16[768,4,64]{0,2,1:T(8,128)(2,1)S(1)} %get-tuple-element.222), kind=kOutput, calls=%fused_computation.123.clone.1 | convolution fusion | flops 402653184 | bytes 13500416 | tf_op jit(solution)/shard_map/while/body/eval_jaxpr/qhd,khd->hqk/dot_general | solution.py:59
  247.8 6.4 %fusion.130 = (f32[4,768]{1,0:T(4,128)S(1)}, f32[4,768,1024]{1,2,0:T(8,128)S(1)}) fusion(bf16[768,4,32]{0,2,1:T(8,128)(2,1)S(1)} %get-tuple-element.224, bf16[6,1024,32]{1,2,0:T(8,128)(2,1)} %get-tuple-element.223, s32[]{:T(128)S(6)} %copy.51, f32[4,1024,768]{2,1,0:T(8,128)} %fusion.129), kind=kOutput, calls=%fused_computation.121.clone.1 | convolution fusion | flops 210760704 | bytes 25440260 | tf_op jit(solution)/shard_map/while/body/eval_jaxpr/qhr,kr->hqk/dot_general | solution.py:60
  255.9 2.3 fusion.134
  261.1 6.3 %fusion.129 = f32[4,1024,768]{2,1,0:T(8,128)} fusion(bf16[1024,4,64]{0,2,1:T(8,128)(2,1)S(1)} %bitcast.107, bf16[768,4,64]{0,2,1:T(8,128)(2,1)S(1)} %get-tuple-element.222), kind=kOutput, calls=%fused_computation.123.clone.1 | convolution fusion | flops 402653184 | bytes 13500416 | tf_op jit(solution)/shard_map/while/body/eval_jaxpr/qhd,khd->hqk/dot_general | solution.py:59
  267.5 6.4 %fusion.130 = (f32[4,768]{1,0:T(4,128)S(1)}, f32[4,768,1024]{1,2,0:T(8,128)S(1)}) fusion(bf16[768,4,32]{0,2,1:T(8,128)(2,1)S(1)} %get-tuple-element.224, bf16[6,1024,32]{1,2,0:T(8,128)(2,1)} %get-tuple-element.223, s32[]{:T(128)S(6)} %copy.51, f32[4,1024,768]{2,1,0:T(8,128)} %fusion.129), kind=kOutput, calls=%fused_computation.121.clone.1 | convolution fusion | flops 210760704 | bytes 25440260 | tf_op jit(solution)/shard_map/while/body/eval_jaxpr/qhr,kr->hqk/dot_general | solution.py:60
  275.6 2.3 fusion.134
  280.1 5.9 %add_convert_fusion = bf16[768,2048]{1,0:T(8,128)(2,1)} fusion(f32[768,2048]{1,0:T(8,128)} %fusion.91, bf16[768,256]{0,1:T(8,128)(2,1)S(1)} %bitcast.114, bf16[256,2048]{1,0:T(8,128)(2,1)} %param.33), kind=kOutput, calls=%fused_computation.25 | convolution fusion | flops 808452096 | bytes 10878976 | tf_op jit(solution)/shard_map/dot_general | solution.py:216
  286.0 36.6 %reduce-scatter.2.cloned.1.call-done = bf16[192,2048]{1,0:T(8,128)(2,1)} async-done(((bf16[768,2048]{1,0:T(8,128)(2,1)}), bf16[192,2048]{1,0:T(8,128)(2,1)}) %reduce-scatter.2.cloned.1.call-update) | async-done | bytes 786448 | tf_op jit(solution)/shard_map/reduce_scatter | solution.py:213
  (173 shorter events, 49.8 us)
Async XLA Ops:
  6.5 95.6 %copy-start = (bf16[2048,768]{1,0:T(8,128)(2,1)S(1)}, bf16[2048,768]{1,0:T(8,128)(2,1)}, u32[]{:S(2)}) copy-start(bf16[2048,768]{1,0:T(8,128)(2,1)} %param.24) | copy-start | bytes 9437188
  6.5 36.4 %copy-start.25 = (f32[2048]{0:T(1024)S(1)}, f32[2048]{0:T(1024)}, u32[]{:S(2)}) copy-start(f32[2048]{0:T(1024)} %param.19) | copy-start | bytes 24580
  6.5 33.6 %all-gather.3.cloned.1.call-start = ((), (), s32[]{:S(2)}) async-start(), calls=%async_computation.1 | async-start | bytes 3932160 | tf_op jit(solution)/shard_map/all_gather | solution.py:108
  7.3 144.7 %all-gather.5.cloned.1.call-start = ((), (), s32[]{:S(2)}) async-start(), calls=%async_computation.2 | async-start | bytes 7077888 | tf_op jit(solution)/shard_map/all_gather | solution.py:203
  40.2 2.8 copy-start.6
  43.0 3.5 %copy-start.16 = (f32[768]{0:T(1024)}, f32[768]{0:T(1024)S(1)}, u32[]{:S(2)}) copy-start(f32[768]{0:T(1024)S(1)} %add_rsqrt_fusion.2) | copy-start | bytes 9220
  43.0 3.6 %copy-start.22 = (bf16[512,256]{1,0:T(8,128)(2,1)S(1)}, bf16[512,256]{1,0:T(8,128)(2,1)}, u32[]{:S(2)}) copy-start(bf16[512,256]{1,0:T(8,128)(2,1)} %param.31) | copy-start | bytes 786436
  43.0 3.6 %copy-start.28 = (f32[512]{0:T(512)S(1)}, f32[512]{0:T(512)}, u32[]{:S(2)}) copy-start(f32[512]{0:T(512)} %param.28) | copy-start | bytes 6148
  43.0 4.1 %copy-start.23 = (bf16[512,256]{1,0:T(8,128)(2,1)S(1)}, bf16[512,256]{1,0:T(8,128)(2,1)}, u32[]{:S(2)}) copy-start(bf16[512,256]{1,0:T(8,128)(2,1)} %param.30) | copy-start | bytes 786436
  46.6 2.1 copy-start.29
  48.6 274.0 %reduce-scatter.2.cloned.1.call-start = ((), (), s32[]{:S(2)}) async-start(), calls=%async_computation.3 | async-start | bytes 3932160 | tf_op jit(solution)/shard_map/reduce_scatter | solution.py:213
  48.8 2.3 copy-start.7
  48.8 2.3 copy-start.20
  49.5 3.5 %copy-start.17 = (f32[768]{0:T(1024)S(1)}, f32[768]{0:T(1024)}, u32[]{:S(2)}) copy-start(f32[768]{0:T(1024)} %copy-done.16) | copy-start | bytes 9220
  49.5 3.5 %copy-start.21 = (bf16[2048,128]{1,0:T(8,128)(2,1)S(1)}, bf16[2048,128]{1,0:T(8,128)(2,1)}, u32[]{:S(2)}) copy-start(bf16[2048,128]{1,0:T(8,128)(2,1)} %param.21) | copy-start | bytes 1572868
  49.5 3.5 %copy-start.26 = (f32[2048]{0:T(1024)S(1)}, f32[2048]{0:T(1024)}, u32[]{:S(2)}) copy-start(f32[2048]{0:T(1024)} %param.19) | copy-start | bytes 24580
  53.0 8.2 %copy-start.9 = (bf16[768,128]{0,1:T(8,128)(2,1)}, bf16[768,128]{0,1:T(8,128)(2,1)S(1)}, u32[]{:S(2)}) copy-start(bf16[768,128]{0,1:T(8,128)(2,1)S(1)} %fusion.52) | copy-start | bytes 589828
  53.0 7.2 %copy-start.24 = (bf16[2048,32]{0,1:T(8,128)(2,1)S(1)}, bf16[2048,32]{0,1:T(8,128)(2,1)}, u32[]{:S(2)}) copy-start(bf16[2048,32]{0,1:T(8,128)(2,1)} %param.26) | copy-start | bytes 393220
  54.2 43.2 %copy-start.11 = (bf16[768,128]{0,1:T(8,128)(2,1)}, bf16[768,128]{0,1:T(8,128)(2,1)S(1)}, u32[]{:S(2)}) copy-start(bf16[768,128]{0,1:T(8,128)(2,1)S(1)} %fusion.55) | copy-start | bytes 589828
  54.3 43.2 %copy-start.18 = (bf16[2048,256]{1,0:T(8,128)(2,1)S(1)}, bf16[2048,256]{1,0:T(8,128)(2,1)}, u32[]{:S(2)}) copy-start(bf16[2048,256]{1,0:T(8,128)(2,1)} %param.20) | copy-start | bytes 3145732
  54.9 53.0 %collective-permute-start = (bf16[128,256]{0,1:T(8,128)(2,1)}, bf16[128,256]{0,1:T(8,128)(2,1)}, u32[]{:S(2)}, u32[]{:S(2)}) collective-permute-start(bf16[128,256]{0,1:T(8,128)(2,1)} %get-tuple-element.122), channel_id=1, source_target_pairs={{0,4},{4,8},{8,12},{12,16},{16,20},{20,24},{24,28},{1,5},{5,9},{9,... | collective-permute-start | bytes 196616 | tf_op jit(solution)/shard_map/ppermute | solution.py:28
  58.9 49.0 %collective-permute-start.1 = (bf16[128,256]{0,1:T(8,128)(2,1)}, bf16[128,256]{0,1:T(8,128)(2,1)}, u32[]{:S(2)}, u32[]{:S(2)}) collective-permute-start(bf16[128,256]{0,1:T(8,128)(2,1)} %get-tuple-element.123), channel_id=1, source_target_pairs={{4,0},{8,4},{12,8},{16,12},{20,16},{24,20},{28,24},{5,1},{9,5},{13... | collective-permute-start | bytes 196616 | tf_op jit(solution)/shard_map/ppermute | solution.py:29
  102.1 4.8 %copy-start.19 = (bf16[768,384]{1,0:T(8,128)(2,1)S(1)}, bf16[768,384]{1,0:T(8,128)(2,1)}, u32[]{:S(2)}) copy-start(bf16[768,384]{1,0:T(8,128)(2,1)} %param.29) | copy-start | bytes 1769476
  102.1 4.8 %copy-start.27 = (f32[768]{0:T(1024)S(1)}, f32[768]{0:T(1024)}, u32[]{:S(2)}) copy-start(f32[768]{0:T(1024)} %param.27) | copy-start | bytes 9220
  107.7 1.7 copy-start.2
  107.7 1.9 copy-start.5
  113.2 2.5 copy-start.8
  119.3 41.4 %copy-start.13 = (f32[4,768]{1,0:T(4,128)S(1)}, f32[4,768]{1,0:T(4,128)}, u32[]{:S(2)}) copy-start(f32[4,768]{1,0:T(4,128)} %custom-call.1) | copy-start | bytes 36868
  214.8 1.7 copy-start.3
  234.5 1.7 copy-start.3
  254.2 1.7 copy-start.3
  280.1 42.5 %copy-start.1 = (bf16[2048,768]{1,0:T(8,128)(2,1)S(1)}, bf16[2048,768]{1,0:T(8,128)(2,1)}, u32[]{:S(2)}) copy-start(bf16[2048,768]{1,0:T(8,128)(2,1)} %param.24) | copy-start | bytes 9437188
  (13 other events, 14.8 us)
Sparse Core Ops, SparseCore 0:
  8.9 31.2 all-gather.2
  48.7 103.2 all-gather.4
  286.1 36.4 reduce-scatter.1
where the time goes:
time: 330 us; the launch traced here: 329 us
  matrix products  120 us (36%)
  waiting for transfers between devices  103 us (31%)
  blocking collectives  34.6 us (10%)
  local copies, waits for them, and re-layouts  30.6 us (9%)
  other arithmetic  21.8 us (7%)
  between operations  13.6 us (4%)
  starting transfers between devices  5.34 us (2%)
    dot_general x6, matrix products, attend(): jnp.einsum('qhr,kr->hqk', q_rot, rot_keys, preferred_element_type=jnp.flo...  38.7 us
    dot_general x6, matrix products, attend(): jnp.einsum('qhd,khd->hqk', q_nope, key_rows, preferred_element_type=jnp.f...  38.1 us
    reduce_scatter x1, waiting for transfers between devices, per_device(): lax.psum_scatter((jnp.dot(out_window, window_out, preferred_element_type=...  36.6 us
    all_gather x1, blocking collectives, per_device(): lax.all_gather(k_rot, 'sp', axis=0, tiled=True)  34.6 us
    all_gather x1, waiting for transfers between devices, per_device(): lax.all_gather(tokens, 'tp', axis=1, tiled=True).astype(jnp.float32)  32.9 us
    all_gather x1, waiting for transfers between devices, per_device(): lax.all_gather(paired, 'sp', axis=0, tiled=True)  32.7 us
    dot_general x6, matrix products, per_device(): updated.append(jnp.dot(scaled, weight, preferred_element_type=jnp.float32))  14.1 us
    dot_general x6, matrix products, attend(): jnp.einsum('hqk,khd->qhd', weights.astype(jnp.bfloat16), value_rows, pref...  13.7 us
  transfers between devices with their start and end apart: 5, of which 3 were waited for; matrix products, arithmetic and copies ran while one was open for 9% of the time, Pallas kernels for 0%

commit v1 on v0

v1 whole, which is shorter than its diff:
```python
import functools

import jax
import jax.numpy as jnp
from jax import lax
from jax.experimental import pallas as pl
from jax.experimental.pallas import tpu as pltpu
from jax.sharding import PartitionSpec as P

A_HEADS = 16
HD = 64
NOPE = 64
ROPE = 32
VD = 64
WINDOW = 128

EPS = 1e-06
THETA = 10000.0
LANES = 128
QCOLS = 256
NEG = -1e30
LOG2E = 1.4426950408889634
F32 = jnp.float32
BF16 = jnp.bfloat16


def swap(x, bit):
    size = lax.axis_size("tp")
    return lax.ppermute(x, "tp", [(i, i ^ bit) for i in range(size)])


def norm_rows(values, gain_vec):
    as_float = values.astype(F32)
    return (
        as_float * lax.rsqrt(jnp.mean(as_float * as_float, axis=1, keepdims=True) + EPS) * gain_vec
    ).astype(BF16)


def angle_table(positions, half_len):
    inverse = THETA ** (-jnp.arange(half_len, dtype=F32) / half_len)
    angles = inverse[:, None] * positions.astype(F32)[None, :]
    return jnp.cos(angles), jnp.sin(angles)


def flash_kernel(scale, chunk, run, started, last, *refs):
    refs = list(refs)
    k_ref, rot_ref, v_ref, q_ref = refs[:4]
    state = refs[4:6] if started else None
    outs = refs[4 + (2 if started else 0) : -2]
    keys, values_t = refs[-2:]

    @pl.when(lax.rem(pl.program_id(0), run) == 0)
    def _():
        keys[:, :LANES] = k_ref[...]
        keys[:, LANES:] = rot_ref[...]
        values_t[...] = v_ref[...].T

    count = keys.shape[0] // chunk
    factor = scale * LOG2E
    q = q_ref[...]

    def score(i):
        return jnp.dot(keys[i * chunk : (i + 1) * chunk, :], q, preferred_element_type=F32)

    top = total = acc = None
    if started:
        top, total, acc = state[0][0:1, :], state[0][1:2, :], state[1][...]
    pending = score(0)
    for i in range(count):
        s = pending
        if i + 1 < count:
            pending = score(i + 1)
        best = jnp.max(s, axis=0, keepdims=True)
        new_top = best if top is None else jnp.maximum(top, best)
        p = jnp.exp2(s * factor - new_top * factor)
        part = jnp.sum(p, axis=0, keepdims=True)
        mixed = jnp.dot(
            values_t[:, i * chunk : (i + 1) * chunk], p.astype(BF16), preferred_element_type=F32
        )
        if top is None:
            total, acc = part, mixed
        else:
            rescale = jnp.exp2((top - new_top) * factor)
            total = total * rescale + part
            acc = acc * rescale + mixed
        top = new_top
    if last:
        outs[0][...] = (acc / total).T.astype(BF16)
    else:
        outs[0][0:1, :] = top
        outs[0][1:2, :] = total
        outs[1][...] = acc


def flash(keys, rot, values, q_cols, state, pairs, chunk, scale, base=0, cols=None):
    last = cols is not None
    rows, cols = keys.shape[0], cols or q_cols.shape[1]
    step = QCOLS
    run = q_cols.shape[1] // (2 * pairs * step)
    first = base // step
    pair = lambda n: (0, lax.rem(lax.div(n, run), pairs))
    column = lambda n: (0, n + first)
    in_specs = [
        pl.BlockSpec((rows, LANES), pair),
        pl.BlockSpec((rows, LANES), lambda n: (0, 0)),
        pl.BlockSpec((rows, LANES), pair),
        pl.BlockSpec((2 * LANES, step), column),
    ]
    if state is not None:
        in_specs += [pl.BlockSpec((8, step), column), pl.BlockSpec((LANES, step), column)]
    if last:
        out_specs = pl.BlockSpec((step, LANES), lambda n: (n, 0))
        out_shape = jax.ShapeDtypeStruct((cols, LANES), BF16)
    else:
        out_specs = [pl.BlockSpec((8, step), column), pl.BlockSpec((LANES, step), column)]
        out_shape = [
            jax.ShapeDtypeStruct((8, cols), F32),
            jax.ShapeDtypeStruct((LANES, cols), F32),
        ]
    return pl.pallas_call(
        functools.partial(flash_kernel, scale, chunk, run, state is not None, last),
        grid=(cols // step,),
        in_specs=in_specs,
        out_specs=out_specs,
        out_shape=out_shape,
        scratch_shapes=[pltpu.VMEM((rows, 2 * LANES), BF16), pltpu.VMEM((LANES, rows), BF16)],
        compiler_params=pltpu.CompilerParams(
            dimension_semantics=("arbitrary",), vmem_limit_bytes=40 * 1024 * 1024
        ),
        cost_estimate=pl.CostEstimate(
            flops=2 * rows * cols * 4 * LANES,
            transcendentals=rows * cols,
            bytes_accessed=rows * 5 * LANES * 2 + cols * 8 * LANES,
        ),
        name="latent_flash",
    )(keys, rot, values, q_cols, *(state or ()))


def window_kernel(
    heads, kv_heads, half, info_ref, slope_ref, sink_ref, q_ref, k_ref, v_ref, out_ref
):
    which = info_ref[pl.program_id(0)]
    base = pl.multiple_of(which * half, half)
    span = half + 2 * WINDOW
    keys = k_ref[pl.ds(base, span), :]
    values_t = v_ref[pl.ds(base, span), :].T
    q_t = q_ref[...].T
    row = lax.broadcasted_iota(jnp.int32, (span, half), 0)
    col = lax.broadcasted_iota(jnp.int32, (span, half), 1)
    distance = jnp.abs(col + WINDOW - row)
    key_pos = info_ref[2] + base + row - WINDOW
    valid = (distance <= WINDOW) & (key_pos >= 0) & (key_pos < info_ref[3])
    apart = distance.astype(F32)
    group = heads // kv_heads
    outs = []
    for h in range(heads):
        g = h // group
        mine = q_t[h * HD : (h + 1) * HD, :]
        pieces = [mine if i == g else jnp.zeros_like(mine) for i in range(kv_heads)]
        weight = pieces[0] if kv_heads == 1 else jnp.concatenate(pieces, axis=0)
        s = jnp.dot(keys, weight, preferred_element_type=F32) * HD ** (-0.5)
        s = jnp.where(valid, s - slope_ref[h] * apart, NEG)
        sink = sink_ref[h]
        top = jnp.maximum(jnp.max(s, axis=0, keepdims=True), sink)
        p = jnp.exp(s - top)
        denom = jnp.sum(p, axis=0, keepdims=True) + jnp.exp(sink - top)
        p = (p * (1.0 / denom)).astype(BF16)
        mixed = jnp.dot(values_t, p, preferred_element_type=F32)
        outs.append(mixed[g * HD : (g + 1) * HD, :])
    out_ref[...] = jnp.concatenate(outs, axis=0).T.astype(BF16)


def window_attention(q, k_pad, v_pad, info, slopes, sinks):
    rows, width = q.shape
    half = rows // 2
    heads, kv_heads = width // HD, k_pad.shape[1] // HD
    whole = lambda n, info: (0, 0)
    smem = pl.BlockSpec(memory_space=pltpu.SMEM)
    return pl.pallas_call(
        functools.partial(window_kernel, heads, kv_heads, half),
        grid_spec=pltpu.PrefetchScalarGridSpec(
            num_scalar_prefetch=1,
            grid=(2,),
            in_specs=[
                smem,
                smem,
                pl.BlockSpec((half, width), lambda n, info: (info[n], 0)),
                pl.BlockSpec(k_pad.shape, whole),
                pl.BlockSpec(v_pad.shape, whole),
            ],
            out_specs=pl.BlockSpec((half, width), lambda n, info: (n, 0)),
        ),
        out_shape=jax.ShapeDtypeStruct((rows, width), BF16),
        compiler_params=pltpu.CompilerParams(
            dimension_semantics=("arbitrary",), vmem_limit_bytes=40 * 1024 * 1024
        ),
        cost_estimate=pl.CostEstimate(
            flops=8 * rows * 640 * width,
            transcendentals=rows * 640 * heads,
            bytes_accessed=rows * width * 8,
        ),
        name="window_flash",
    )(info, slopes, sinks, q, k_pad, v_pad)


def per_device(
    tokens,
    norm_gain,
    window_query,
    window_key,
    window_value,
    sink_logit,
    down_query,
    down_latent,
    rotary_proj,
    query_gain,
    latent_gain,
    up_query,
    up_key,
    up_value,
    window_out,
    latent_out,
):
    rows, part = tokens.shape
    tp_size, tp = lax.axis_size("tp"), lax.axis_index("tp")
    sp_size, sp = lax.axis_size("sp"), lax.axis_index("sp")
    top_bit = tp_size // 2
    half = rows // 2
    width = part * tp_size

    def near(block):
        blocks, bit = [block], 1
        while bit < top_bit:
            blocks = blocks + [swap(b, bit) for b in blocks]
            bit *= 2
        return blocks

    far_block = swap(tokens, top_bit)
    groups = [near(tokens), near(far_block)]
    projections = (down_latent, down_query, window_query, window_key, window_value, rotary_proj)
    joined = jnp.concatenate(projections, axis=1)

    squares, acc = None, None
    for g, blocks in enumerate(groups):
        starts = [(tp ^ (g * top_bit + k)) * part for k in range(top_bit)]
        weight = jnp.concatenate([lax.dynamic_slice_in_dim(joined, s, part, 0) for s in starts])
        gain = jnp.concatenate([lax.dynamic_slice_in_dim(norm_gain, s, part, 0) for s in starts])
        as_float = jnp.concatenate(blocks, axis=1).astype(F32)
        scaled = (as_float * gain[None, :]).astype(BF16)
        square = jnp.sum(as_float * as_float, axis=1)
        product = jnp.dot(scaled, weight, preferred_element_type=F32)
        squares = square if squares is None else squares + square
        acc = product if acc is None else acc + product
    row_scale = lax.rsqrt(squares / width + EPS)[:, None]
    outs, at = [], 0
    for weight in projections:
        outs.append((acc[:, at : at + weight.shape[1]] * row_scale).astype(BF16))
        at += weight.shape[1]
    latent_kv, latent_q, q_window, k_window, v_window, rotary_rows = outs

    first_pos = sp * rows
    positions = first_pos + jnp.arange(rows, dtype=jnp.int32)
    half_rope = ROPE // 2
    cosine, sine = angle_table(positions, half_rope)
    front, back = rotary_rows[:, :half_rope].astype(F32), rotary_rows[:, half_rope:].astype(F32)
    cos_k, sin_k = cosine.T, sine.T
    k_rot = jnp.concatenate(
        [
            front * cos_k - back * sin_k,
            back * cos_k + front * sin_k,
            jnp.zeros((rows, LANES - ROPE), F32),
        ],
        axis=1,
    ).astype(BF16)
    normed_kv = norm_rows(latent_kv, latent_gain)
    core = tp % 2
    kv_half = latent_kv.shape[1] // 2
    piece = lax.dynamic_slice_in_dim(normed_kv, core * kv_half, kv_half, 1)
    ring = [(i, (i + 2) % sp_size) for i in range(sp_size)]
    side = [(i, i ^ 1) for i in range(sp_size)]
    up_both = jnp.concatenate([up_key, up_value], axis=1)
    up_both = jnp.concatenate(
        [
            lax.dynamic_slice_in_dim(up_both, core * kv_half, kv_half, 0),
            lax.dynamic_slice_in_dim(up_both, (1 - core) * kv_half, kv_half, 0),
        ]
    )
    latent_heads = up_query.shape[1] // (NOPE + ROPE)
    pairs = latent_heads // 2
    payload = jnp.concatenate([piece, k_rot], axis=1)
    arrived = []
    for i in range(sp_size // 2):
        both = jnp.concatenate([payload, lax.ppermute(payload, "sp", side)], axis=0)
        arrived.append((both[:, :kv_half], swap(both[:, :kv_half], 1), both[:, kv_half:]))
        if i + 1 < sp_size // 2:
            payload = lax.ppermute(payload, "sp", ring)

    top_set = tp // top_bit
    other = 1 - top_set
    heads_dev = window_query.shape[1] // HD
    stacked = jnp.concatenate([k_window, v_window], axis=1)
    up = [(i, i + 1) for i in range(sp_size - 1)]
    down = [(i + 1, i) for i in range(sp_size - 1)]
    before = lax.ppermute(stacked[rows - WINDOW :], "sp", up)
    after = lax.ppermute(stacked[:WINDOW], "sp", down)
    padded = jnp.concatenate([before, stacked, after], axis=0)
    kv_width = k_window.shape[1]
    head_ids = tp * heads_dev + jnp.arange(heads_dev, dtype=jnp.int32)
    slopes = jnp.exp2(-8.0 * (head_ids.astype(F32) + 1.0) / A_HEADS)
    info = jnp.stack([other, top_set, first_pos, rows * sp_size]).astype(jnp.int32)
    out_window = window_attention(
        q_window, padded[:, :kv_width], padded[:, kv_width:], info, slopes, sink_logit
    )

    def reorder(x):
        return jnp.concatenate(
            [
                lax.dynamic_slice_in_dim(x, other * half, half, 0),
                lax.dynamic_slice_in_dim(x, top_set * half, half, 0),
            ],
            axis=0,
        )

    normed_q = norm_rows(reorder(latent_q), query_gain)
    q_t = lax.dot_general(
        up_query, normed_q, (((0,), (1,)), ((), ())), preferred_element_type=F32
    ).astype(BF16)
    q_t = q_t.reshape(latent_heads, NOPE + ROPE, rows)
    cos_q, sin_q = angle_table(reorder(positions), half_rope)
    q_front = q_t[:, NOPE : NOPE + half_rope].astype(F32)
    q_back = q_t[:, NOPE + half_rope :].astype(F32)
    q_rot = jnp.concatenate(
        [q_front * cos_q - q_back * sin_q, q_back * cos_q + q_front * sin_q], axis=1
    ).astype(BF16)
    zeros_head = jnp.zeros((NOPE, half), BF16)
    zeros_tail = jnp.zeros((LANES - ROPE, half), BF16)

    def columns(p, part_at):
        span = slice(part_at * half, (part_at + 1) * half)
        both = []
        for j in range(2):
            h = 2 * p + j
            nope = [q_t[h, :NOPE, span], zeros_head]
            both.append(
                jnp.concatenate(
                    (nope if j == 0 else nope[::-1]) + [q_rot[h, :, span], zeros_tail], axis=0
                )
            )
        return jnp.concatenate(both, axis=1)

    q_cols = jnp.concatenate(
        [columns(p, at) for at in range(2) for p in range(pairs)], axis=1
    )
    lat_scale = (NOPE + ROPE) ** (-0.5)
    lane = lax.broadcasted_iota(jnp.int32, (half, LANES), 1)
    halves = [[], []]
    state = None
    for i, (mine, theirs, rot) in enumerate(arrived):
        expanded = jnp.dot(
            jnp.concatenate([mine, theirs], axis=1), up_both, preferred_element_type=F32
        ).astype(BF16)
        keys, values = expanded[:, : pairs * LANES], expanded[:, pairs * LANES :]
        args = (keys, rot, values, q_cols, state, pairs, rows, lat_scale)
        if i + 1 < len(arrived):
            state = flash(*args)
            continue
        size = q_cols.shape[1] // 2
        for at in range(2):
            r = flash(*args, base=at * size, cols=size)
            for p in range(pairs):
                start = p * 2 * half
                first, second = r[start : start + half], r[start + half : start + 2 * half]
                halves[at].append(jnp.where(lane < VD, first, second))

    weight_out = jnp.concatenate([window_out, latent_out], axis=0)

    def project(x):
        return jnp.dot(x, weight_out, preferred_element_type=F32).astype(BF16)

    def reduce_near(x):
        bit = top_bit // 2
        if bit == 0:
            return project(x).astype(F32)
        count = x.shape[0] // 2
        mine = (tp // bit) % 2
        sent = project(lax.dynamic_slice_in_dim(x, (1 - mine) * count, count, 0))
        got = swap(sent, bit)
        total = project(lax.dynamic_slice_in_dim(x, mine * count, count, 0)).astype(F32)
        total = total + got.astype(F32)
        bit //= 2
        while bit:
            count //= 2
            mine = (tp // bit) % 2
            sent = lax.dynamic_slice_in_dim(total, (1 - mine) * count, count, 0).astype(BF16)
            total = lax.dynamic_slice_in_dim(total, mine * count, count, 0)
            total = total + swap(sent, bit).astype(F32)
            bit //= 2
        return total

    inputs = [
        jnp.concatenate([out_window[at * half : (at + 1) * half]] + halves[at], axis=1)
        for at in range(2)
    ]
    far_total = swap(reduce_near(inputs[0]).astype(BF16), top_bit)
    return (reduce_near(inputs[1]) + far_total.astype(F32)).astype(BF16)


def solution(mesh):
    placed = (
        P("sp", "tp"),
        P(),
        P(None, "tp"),
        P(None, "tp"),
        P(None, "tp"),
        P("tp"),
        P(),
        P(),
        P(),
        P(),
        P(),
        P(None, "tp"),
        P(None, "tp"),
        P(None, "tp"),
        P("tp", None),
        P("tp", None),
    )
    return jax.shard_map(
        per_device, mesh=mesh, in_specs=placed, out_specs=P(("sp", "tp"), None), check_vma=False
    )
```

time: 330 us -> 176 us (0.53)
  matrix products: 120 us -> 17.4 us
  waiting for transfers between devices: 103 us -> 43.1 us
  Pallas kernels: 0 us -> 59.5 us
  blocking collectives: 34.6 us -> 0 us
  starting transfers between devices: 5.34 us -> 19 us
  between operations: 13.6 us -> 0.81 us
  other arithmetic: 21.8 us -> 12.1 us
  local copies, waits for them, and re-layouts: 30.6 us -> 23.2 us
    dot_general x31 -> x11, matrix products: 120 us -> 17.4 us  [the longest x2 9.17 us: per_device(): product = jnp.dot(scaled, weight, preferred_element_type=F32)]
    all_gather x2 -> x0, waiting for transfers between devices: 65.6 us -> none  [the longest x1 32.9 us: per_device(): lax.all_gather(tokens, 'tp', axis=1, tiled=True).astype(jnp.float32)]
    pallas_call x0 -> x6, Pallas kernels: none -> 59.5 us  [the longest x5 53.2 us: flash(): pl.pallas_call(functools.partial(flash_kernel, scale, chunk, run, state i...]
    ppermute x2 -> x19, waiting for transfers between devices: 0.01 us -> 43.1 us  [the longest x10 18.9 us: swap(): return lax.ppermute(x, 'tp', [(i, i ^ bit) for i in range(size)])]
    reduce_scatter x1 -> x0, waiting for transfers between devices: 36.6 us -> none  [per_device(): lax.psum_scatter((jnp.dot(out_window, window_out, preferred_element_type=...]
    all_gather x1 -> x0, blocking collectives: 34.6 us -> none  [per_device(): lax.all_gather(k_rot, 'sp', axis=0, tiled=True)]
    ppermute x2 -> x19, starting transfers between devices: 5.26 us -> 19 us  [the longest x4 7.97 us: per_device(): both = jnp.concatenate([payload, lax.ppermute(payload, 'sp', side)], axis=0)]
    unnamed x57 -> x43, local copies, waits for them, and re-layouts: 0.78 us -> 12.7 us
  transfers between devices with their start and end apart: 5 -> 19, of which waited for: 3 -> 7; matrix products, arithmetic and copies ran while one was open for 9% -> 23% of each run, Pallas kernels for 0% -> 26%
where the time goes in v1:
time: 176 us; the launch traced here: 175 us
  Pallas kernels  59.5 us (34%)
  waiting for transfers between devices  43.1 us (24%)
  local copies, waits for them, and re-layouts  23.2 us (13%)
  starting transfers between devices  19 us (11%)
  matrix products  17.4 us (10%)
  other arithmetic  12.1 us (7%)
    pallas_call x5, Pallas kernels, flash(): pl.pallas_call(functools.partial(flash_kernel, scale, chunk, run, state i...  53.2 us
    ppermute x10, waiting for transfers between devices, swap(): return lax.ppermute(x, 'tp', [(i, i ^ bit) for i in range(size)])  18.9 us
    unnamed x43, local copies, waits for them, and re-layouts  12.7 us
    ppermute x4, waiting for transfers between devices, per_device(): both = jnp.concatenate([payload, lax.ppermute(payload, 'sp', side)], axis=0)  12.4 us
    dot_general x2, matrix products, per_device(): product = jnp.dot(scaled, weight, preferred_element_type=F32)  9.17 us
    ppermute x4, starting transfers between devices, per_device(): both = jnp.concatenate([payload, lax.ppermute(payload, 'sp', side)], axis=0)  7.97 us
    ppermute x1, waiting for transfers between devices, per_device(): before = lax.ppermute(stacked[rows - WINDOW:], 'sp', up)  6.64 us
    pallas_call x1, Pallas kernels, window_attention(): pl.pallas_call(functools.partial(window_kernel, heads, kv_heads, half), g...  6.27 us
  transfers between devices with their start and end apart: 19, of which 7 were waited for; matrix products, arithmetic and copies ran while one was open for 23% of the time, Pallas kernels for 26%

profile of v1, /device:TPU:0, one launch (start us, length us, event | category | flops | bytes accessed | tf_op | source)
XLA Modules:
  0.0 175.0 jit_solution(12625510895423125250)
XLA Ops:
  0.5 2.6 %collective-permute-start.1 = (bf16[768,512]{1,0:T(8,128)(2,1)}, bf16[768,512]{1,0:T(8,128)(2,1)}, u32[]{:S(2)}, u32[]{:S(2)}) collective-permute-start(bf16[768,512]{1,0:T(8,128)(2,1)} %param.16), channel_id=1, source_target_pairs={{0,2},{1,3},{2,0},{3,1},{4,6},{5,7},{6,4},{7,5},{8,10},{9,11},{10,... | collective-permute-start | bytes 2359304 | tf_op jit(solution)/shard_map/ppermute | solution.py:29
  3.1 3.2 %constant_dynamic-update-slice_fusion.5 = bf16[2048,1824]{1,0:T(8,128)(2,1)} fusion(bf16[2048,512]{1,0:T(8,128)(2,1)} %param.23), kind=kLoop, calls=%fused_computation.159 | loop fusion | bytes 4194304
  7.4 1.3 constant_dynamic-update-slice_fusion.15
  8.8 3.9 %constant_dynamic-update-slice_fusion.4 = bf16[2048,1824]{1,0:T(8,128)(2,1)} fusion(bf16[2048,1824]{1,0:T(8,128)(2,1)} %constant_dynamic-update-slice_fusion.5, bf16[2048,768]{1,0:T(8,128)(2,1)} %param.22), kind=kLoop, calls=%fused_computation.158 | loop fusion | bytes 6291456
  12.7 1.1 constant_dynamic-update-slice_fusion.3
  17.4 1.3 constant_dynamic-update-slice_fusion.14
  21.3 4.0 %constant_dynamic-slice_fusion.5 = (bf16[512,1824]{1,0:T(8,128)(2,1)S(1)}, bf16[512,1824]{1,0:T(8,128)(2,1)S(1)}, bf16[512,1824]{1,0:T(8,128)(2,1)S(1)}, bf16[512,1824]{1,0:T(8,128)(2,1)S(1)}) fusion(bf16[2048,1824]{1,0:T(8,128)(2,1)} %constant_dynamic-update-slice_fusion, s32[]{:T(128)S(6)} %select_n.72, s32[]{:T(128)S(6)} %select_n.73, s32[]{:T(128)S(6)} %select_n.71, ...), kind=kLoop, calls=%fused_computation.210 | loop fusion | bytes 14942224 | tf_op jit(solution)/shard_map/dynamic_slice | solution.py:246
  25.6 1.5 fusion.12
  27.1 4.6 %fusion = f32[768,1824]{1,0:T(8,128)S(1)} fusion(bf16[512,1824]{1,0:T(8,128)(2,1)S(1)} %get-tuple-element.21, bf16[512,1824]{1,0:T(8,128)(2,1)S(1)} %get-tuple-element.22, f32[1024]{0:T(1024)S(1)} %get-tuple-element.77, bf16[768,512]{1,0:T(8,128)(2,1)} %collective-permute-done, bf16[768,512]{1,0:T(8,128)(2,1)S(1)} %copy-done.5), kind=kOutput, calls=%fused_computation | convolution fusion | flops 2881093632 | bytes 10915840 | tf_op jit(solution)/shard_map/dot_general | solution.py:251
  31.7 1.5 fusion.14
  33.2 4.6 %fusion.8 = f32[768,1824]{1,0:T(8,128)S(1)} fusion(f32[768,1824]{1,0:T(8,128)S(1)} %fusion, bf16[512,1824]{1,0:T(8,128)(2,1)S(1)} %get-tuple-element.20, bf16[512,1824]{1,0:T(8,128)(2,1)S(1)} %get-tuple-element.19, f32[1024]{0:T(1024)S(1)} %get-tuple-element.78, bf16[768,512]{1,0:T(8,128)(2,1)S(1)} %collective-permute-done.2, ...), kind=kOutput, calls=%fused_computation.12 | convolution fusion | flops 2882494464 | bytes 16519168 | tf_op jit(solution)/shard_map/dot_general | solution.py:251
  38.9 1.9 %fusion.50 = (bf16[768,16]{1,0:T(8,128)(2,1)S(1)}, bf16[768,16]{1,0:T(8,128)(2,1)S(1)}) fusion(f32[768]{0:T(1024)S(1)} %fusion.109, f32[16]{0:T(128)S(1)} %multiply_power_fusion, bf16[768,32]{1,0:T(8,128)(2,1)S(1)} %fusion.53), kind=kLoop, calls=%fused_computation.84 | loop fusion | flops 135168 | bytes 101440 | tf_op jit(solution)/shard_map/convert.2
  41.2 1.6 collective-permute-start.14
  42.8 1.6 collective-permute-start.5
  44.4 2.4 %collective-permute-start.3 = (bf16[128,256]{1,0:T(8,128)(2,1)S(1)}, bf16[128,256]{1,0:T(8,128)(2,1)S(1)}, u32[]{:S(2)}, u32[]{:S(2)}) collective-permute-start(bf16[128,256]{1,0:T(8,128)(2,1)S(1)} %get-tuple-element.55), channel_id=1, source_target_pairs={{0,4},{4,8},{8,12},{12,16},{16,20},{20,24},{24,28},{1,5},{5,9},{9,... | collective-permute-start | bytes 196616 | tf_op jit(solution)/shard_map/ppermute | solution.py:304
  46.8 1.5 collective-permute-start.4
  50.7 6.6 %collective-permute-done.3 = bf16[128,256]{1,0:T(8,128)(2,1)S(1)} collective-permute-done((bf16[128,256]{1,0:T(8,128)(2,1)S(1)}, bf16[128,256]{1,0:T(8,128)(2,1)S(1)}, u32[]{:S(2)}, u32[]{:S(2)}) %collective-permute-start.3) | collective-permute-done | bytes 65568 | tf_op jit(solution)/shard_map/ppermute | solution.py:304
  58.4 6.3 %window_flash.1 = bf16[768,256]{1,0:T(8,128)(2,1)S(1)} custom-call(s32[4]{0:T(128)S(1)} %pad_add_fusion.info_ref, f32[4]{0:T(128)S(1)} %multiply_exponential_fusion.slope_ref, f32[4]{0:T(128)S(1)} %copy-done.2, bf16[768,256]{1,0:T(8,128)(2,1)S(1)} %fusion.44.q_ref, bf16[1024,128]{1,0:T(8,128)(2,1)S(1)} %get-tuple-element.46.k_ref, ...), custom_call_target="tpu_custom_call" | custom-call | flops 1006632960 | bytes 1572864 | tf_op jit(solution)/shard_map/window_flash/pallas_call | solution.py:179
  65.1 4.6 %collective-permute-start.12 = (bf16[768,384]{1,0:T(8,128)(2,1)S(1)}, bf16[768,384]{1,0:T(8,128)(2,1)S(1)}, u32[]{:S(2)}, u32[]{:S(2)}) collective-permute-start(bf16[768,384]{1,0:T(8,128)(2,1)S(1)} %collective-permute-done.5), channel_id=1, source_target_pairs={{0,4},{4,0},{8,12},{12,8},{16,20},{20,16},{24,28},{28,24},{1,5},{5... | collective-permute-start | bytes 1769480 | tf_op jit(solution)/shard_map/ppermute | solution.py:293
  71.2 12.4 %collective-permute-done.12 = bf16[768,384]{1,0:T(8,128)(2,1)S(1)} collective-permute-done((bf16[768,384]{1,0:T(8,128)(2,1)S(1)}, bf16[768,384]{1,0:T(8,128)(2,1)S(1)}, u32[]{:S(2)}, u32[]{:S(2)}) %collective-permute-start.12) | collective-permute-done | bytes 589856 | tf_op jit(solution)/shard_map/ppermute | solution.py:293
  83.9 3.0 %collective-permute-done.6 = bf16[768,384]{1,0:T(8,128)(2,1)S(1)} collective-permute-done((bf16[768,384]{1,0:T(8,128)(2,1)S(1)}, bf16[768,384]{1,0:T(8,128)(2,1)S(1)}, u32[]{:S(2)}, u32[]{:S(2)}) %collective-permute-start.6) | collective-permute-done | bytes 589856 | tf_op jit(solution)/shard_map/ppermute | solution.py:296
  88.3 13.6 %latent_flash.5 = (f32[8,3072]{1,0:T(8,128)S(1)}, f32[128,3072]{1,0:T(8,128)S(1)}) custom-call(bf16[1536,256]{1,0:T(8,128)(2,1)S(1)} %get-tuple-element.26.refs_0_, bf16[1536,128]{1,0:T(8,128)(2,1)S(1)} %pad_maximum_fusion.18.refs_1_, bf16[1536,256]{1,0:T(8,128)(2,1)S(1)} %get-tuple-element.25.refs_2_, bf16[256,3072]{1,0:T(8,128)(2,1)S(1)} %fusion.83.refs_3_), custom_call_target="tpu_custom_call" | custom-call | flops 4831838208 | bytes 5111808 | tf_op jit(solution)/shard_map/latent_flash/pallas_call | solution.py:120
  102.2 1.2 collective-permute-done.7
  103.4 1.5 collective-permute-start.8
  106.1 13.2 %latent_flash.6 = (f32[8,3072]{1,0:T(8,128)S(1)}, f32[128,3072]{1,0:T(8,128)S(1)}) custom-call(bf16[1536,256]{1,0:T(8,128)(2,1)S(1)} %get-tuple-element.28.refs_0_, bf16[1536,128]{1,0:T(8,128)(2,1)S(1)} %slice.273.refs_1_, bf16[1536,256]{1,0:T(8,128)(2,1)S(1)} %get-tuple-element.27.refs_2_, bf16[256,3072]{1,0:T(8,128)(2,1)S(1)} %fusion.83.refs_3_, ...), custom_call_target="tpu_custom_call" | custom-call | flops 4831838208 | bytes 5111808 | tf_op jit(solution)/shard_map/latent_flash/pallas_call | solution.py:120
  120.6 13.2 %latent_flash.7 = (f32[8,3072]{1,0:T(8,128)S(1)}, f32[128,3072]{1,0:T(8,128)S(1)}) custom-call(bf16[1536,256]{1,0:T(8,128)(2,1)S(1)} %get-tuple-element.30.refs_0_, bf16[1536,128]{1,0:T(8,128)(2,1)S(1)} %slice.269.refs_1_, bf16[1536,256]{1,0:T(8,128)(2,1)S(1)} %get-tuple-element.29.refs_2_, bf16[256,3072]{1,0:T(8,128)(2,1)S(1)} %fusion.83.refs_3_, ...), custom_call_target="tpu_custom_call" | custom-call | flops 4831838208 | bytes 5111808 | tf_op jit(solution)/shard_map/latent_flash/pallas_call | solution.py:120
  133.8 1.0 convolution_convert_fusion.3
  134.9 6.7 %latent_flash.9 = bf16[1536,128]{1,0:T(8,128)(2,1)S(1)} custom-call(bf16[1536,256]{1,0:T(8,128)(2,1)S(1)} %get-tuple-element.32.refs_0_, bf16[1536,128]{1,0:T(8,128)(2,1)S(1)} %slice.240.refs_1_, bf16[1536,256]{1,0:T(8,128)(2,1)S(1)} %get-tuple-element.31.refs_2_, bf16[256,3072]{1,0:T(8,128)(2,1)S(1)} %fusion.83.refs_3_, ...), custom_call_target="tpu_custom_call" | custom-call | flops 2415919104 | bytes 3538944 | tf_op jit(solution)/shard_map/latent_flash/pallas_call | solution.py:120
  141.6 6.7 %latent_flash.8 = bf16[1536,128]{1,0:T(8,128)(2,1)S(1)} custom-call(bf16[1536,256]{1,0:T(8,128)(2,1)S(1)} %get-tuple-element.32.refs_0_, bf16[1536,128]{1,0:T(8,128)(2,1)S(1)} %slice.240.refs_1_, bf16[1536,256]{1,0:T(8,128)(2,1)S(1)} %get-tuple-element.31.refs_2_, bf16[256,3072]{1,0:T(8,128)(2,1)S(1)} %fusion.83.refs_3_, ...), custom_call_target="tpu_custom_call" | custom-call | flops 2415919104 | bytes 3538944 | tf_op jit(solution)/shard_map/latent_flash/pallas_call | solution.py:120
  152.2 1.7 add_convert_fusion.1
  155.1 18.7 %collective-permute-done.18 = bf16[192,2048]{1,0:T(8,128)(2,1)S(1)} collective-permute-done((bf16[192,2048]{1,0:T(8,128)(2,1)S(1)}, bf16[192,2048]{1,0:T(8,128)(2,1)S(1)}, u32[]{:S(2)}, u32[]{:S(2)}) %collective-permute-start.18) | collective-permute-done | bytes 786464 | tf_op jit(solution)/shard_map/ppermute | solution.py:29
  173.8 1.2 add_convert_fusion
  (137 shorter events, 24.2 us)
Async XLA Ops:
  0.0 48.7 %copy-start = (bf16[768,384]{1,0:T(8,128)(2,1)S(1)}, bf16[768,384]{1,0:T(8,128)(2,1)}, u32[]{:S(2)}) copy-start(bf16[768,384]{1,0:T(8,128)(2,1)} %param.27) | copy-start | bytes 1769476
  0.0 25.6 %collective-permute-start = (bf16[768,512]{1,0:T(8,128)(2,1)}, bf16[768,512]{1,0:T(8,128)(2,1)}, u32[]{:S(2)}, u32[]{:S(2)}) collective-permute-start(bf16[768,512]{1,0:T(8,128)(2,1)} %param.16), channel_id=1, source_target_pairs={{0,1},{1,0},{2,3},{3,2},{4,5},{5,4},{6,7},{7,6},{8,9},{9,8},{10,11... | collective-permute-start | bytes 2359304 | tf_op jit(solution)/shard_map/ppermute | solution.py:29
  0.5 24.8 %collective-permute-start.1 = (bf16[768,512]{1,0:T(8,128)(2,1)}, bf16[768,512]{1,0:T(8,128)(2,1)}, u32[]{:S(2)}, u32[]{:S(2)}) collective-permute-start(bf16[768,512]{1,0:T(8,128)(2,1)} %param.16), channel_id=1, source_target_pairs={{0,2},{1,3},{2,0},{3,1},{4,6},{5,7},{6,4},{7,5},{8,10},{9,11},{10,... | collective-permute-start | bytes 2359304 | tf_op jit(solution)/shard_map/ppermute | solution.py:29
  3.1 3.2 %copy-start.13 = (bf16[2048,32]{0,1:T(8,128)(2,1)S(1)}, bf16[2048,32]{0,1:T(8,128)(2,1)}, u32[]{:S(2)}) copy-start(bf16[2048,32]{0,1:T(8,128)(2,1)} %param.24) | copy-start | bytes 393220
  3.1 3.5 %copy-start.10 = (bf16[512,256]{1,0:T(8,128)(2,1)S(1)}, bf16[512,256]{1,0:T(8,128)(2,1)}, u32[]{:S(2)}) copy-start(bf16[512,256]{1,0:T(8,128)(2,1)} %param.28) | copy-start | bytes 786436
  8.8 4.0 %copy-start.4 = (bf16[2048,256]{1,0:T(8,128)(2,1)S(1)}, bf16[2048,256]{1,0:T(8,128)(2,1)}, u32[]{:S(2)}) copy-start(bf16[2048,256]{1,0:T(8,128)(2,1)} %param.18) | copy-start | bytes 3145732
  12.7 2.1 %copy-start.8 = (bf16[2048,128]{1,0:T(8,128)(2,1)S(1)}, bf16[2048,128]{1,0:T(8,128)(2,1)}, u32[]{:S(2)}) copy-start(bf16[2048,128]{1,0:T(8,128)(2,1)} %param.20) | copy-start | bytes 1572868
  12.7 3.0 %copy-start.11 = (bf16[512,256]{1,0:T(8,128)(2,1)S(1)}, bf16[512,256]{1,0:T(8,128)(2,1)}, u32[]{:S(2)}) copy-start(bf16[512,256]{1,0:T(8,128)(2,1)} %param.29) | copy-start | bytes 786436
  15.7 3.8 %copy-start.14 = (f32[2048]{0:T(1024)S(1)}, f32[2048]{0:T(1024)}, u32[]{:S(2)}) copy-start(f32[2048]{0:T(1024)} %param.17) | copy-start | bytes 24580
  16.4 2.3 %copy-start.3 = (bf16[512,512]{1,0:T(8,128)(2,1)S(1)}, bf16[512,512]{1,0:T(8,128)(2,1)}, u32[]{:S(2)}) copy-start(bf16[512,512]{1,0:T(8,128)(2,1)} %constant_dynamic-update-slice_fusion.8) | copy-start | bytes 1572868
  21.3 4.3 %copy-start.5 = (bf16[768,512]{1,0:T(8,128)(2,1)S(1)}, bf16[768,512]{1,0:T(8,128)(2,1)}, u32[]{:S(2)}) copy-start(bf16[768,512]{1,0:T(8,128)(2,1)} %param.16) | copy-start | bytes 2359300
  25.3 6.4 %collective-permute-start.2 = (bf16[768,512]{1,0:T(8,128)(2,1)}, bf16[768,512]{1,0:T(8,128)(2,1)S(1)}, u32[]{:S(2)}, u32[]{:S(2)}) collective-permute-start(bf16[768,512]{1,0:T(8,128)(2,1)} %collective-permute-done.1), channel_id=1, source_target_pairs={{0,1},{1,0},{2,3},{3,2},{4,5},{5,4},{6,7},{7,6},{8,9},{9,8},{10,11... | collective-permute-start | bytes 2359304 | tf_op jit(solution)/shard_map/ppermute | solution.py:29
  41.2 23.4 %collective-permute-start.14 = (bf16[768,384]{1,0:T(8,128)(2,1)S(1)}, bf16[768,384]{1,0:T(8,128)(2,1)S(1)}, u32[]{:S(2)}, u32[]{:S(2)}) collective-permute-start(bf16[768,384]{1,0:T(8,128)(2,1)S(1)} %pad_maximum_fusion.7), channel_id=1, source_target_pairs={{0,4},{4,0},{8,12},{12,8},{16,20},{20,16},{24,28},{28,24},{1,5},{5... | collective-permute-start | bytes 1769480 | tf_op jit(solution)/shard_map/ppermute | solution.py:293
  42.8 22.3 %collective-permute-start.5 = (bf16[768,384]{1,0:T(8,128)(2,1)S(1)}, bf16[768,384]{1,0:T(8,128)(2,1)S(1)}, u32[]{:S(2)}, u32[]{:S(2)}) collective-permute-start(bf16[768,384]{1,0:T(8,128)(2,1)S(1)} %pad_maximum_fusion.7), channel_id=1, source_target_pairs={{0,8},{4,12},{8,16},{12,20},{16,24},{20,28},{24,0},{28,4},{1,9},{5... | collective-permute-start | bytes 1769480 | tf_op jit(solution)/shard_map/ppermute | solution.py:296
  44.3 4.4 %copy-start.15 = (f32[768]{0:T(1024)S(1)}, f32[768]{0:T(1024)}, u32[]{:S(2)}) copy-start(f32[768]{0:T(1024)} %param.25) | copy-start | bytes 9220
  44.4 13.0 %collective-permute-start.3 = (bf16[128,256]{1,0:T(8,128)(2,1)S(1)}, bf16[128,256]{1,0:T(8,128)(2,1)S(1)}, u32[]{:S(2)}, u32[]{:S(2)}) collective-permute-start(bf16[128,256]{1,0:T(8,128)(2,1)S(1)} %get-tuple-element.55), channel_id=1, source_target_pairs={{0,4},{4,8},{8,12},{12,16},{16,20},{20,24},{24,28},{1,5},{5,9},{9,... | collective-permute-start | bytes 196616 | tf_op jit(solution)/shard_map/ppermute | solution.py:304
  46.8 11.4 %collective-permute-start.4 = (bf16[128,256]{1,0:T(8,128)(2,1)S(1)}, bf16[128,256]{1,0:T(8,128)(2,1)S(1)}, u32[]{:S(2)}, u32[]{:S(2)}) collective-permute-start(bf16[128,256]{1,0:T(8,128)(2,1)S(1)} %get-tuple-element.56), channel_id=1, source_target_pairs={{4,0},{8,4},{12,8},{16,12},{20,16},{24,20},{28,24},{5,1},{9,5},{13... | collective-permute-start | bytes 196616 | tf_op jit(solution)/shard_map/ppermute | solution.py:305
  50.0 8.4 %copy-start.2 = (f32[4]{0:T(128)S(1)}, f32[4]{0:T(128)}, u32[]{:S(2)}) copy-start(f32[4]{0:T(128)} %sink_ref.1) | copy-start | bytes 52
  65.0 22.2 %collective-permute-start.15 = (bf16[1536,256]{1,0:T(8,128)(2,1)S(1)}, bf16[1536,256]{1,0:T(8,128)(2,1)S(1)}, u32[]{:S(2)}, u32[]{:S(2)}) collective-permute-start(bf16[1536,256]{1,0:T(8,128)(2,1)S(1)} %slice.275), channel_id=1, source_target_pairs={{0,1},{1,0},{2,3},{3,2},{4,5},{5,4},{6,7},{7,6},{8,9},{9,8},{10,11... | collective-permute-start | bytes 2359304 | tf_op jit(solution)/shard_map/ppermute | solution.py:29
  65.1 18.5 %collective-permute-start.12 = (bf16[768,384]{1,0:T(8,128)(2,1)S(1)}, bf16[768,384]{1,0:T(8,128)(2,1)S(1)}, u32[]{:S(2)}, u32[]{:S(2)}) collective-permute-start(bf16[768,384]{1,0:T(8,128)(2,1)S(1)} %collective-permute-done.5), channel_id=1, source_target_pairs={{0,4},{4,0},{8,12},{12,8},{16,20},{20,16},{24,28},{28,24},{1,5},{5... | collective-permute-start | bytes 1769480 | tf_op jit(solution)/shard_map/ppermute | solution.py:293
  69.7 17.2 %collective-permute-start.6 = (bf16[768,384]{1,0:T(8,128)(2,1)S(1)}, bf16[768,384]{1,0:T(8,128)(2,1)S(1)}, u32[]{:S(2)}, u32[]{:S(2)}) collective-permute-start(bf16[768,384]{1,0:T(8,128)(2,1)S(1)} %collective-permute-done.5), channel_id=1, source_target_pairs={{0,8},{4,12},{8,16},{12,20},{16,24},{20,28},{24,0},{28,4},{1,9},{5... | collective-permute-start | bytes 1769480 | tf_op jit(solution)/shard_map/ppermute | solution.py:296
  83.7 3.5 %copy-start.9 = (bf16[256,512]{1,0:T(8,128)(2,1)S(1)}, bf16[256,512]{1,0:T(8,128)(2,1)}, u32[]{:S(2)}) copy-start(bf16[256,512]{1,0:T(8,128)(2,1)} %get-tuple-element.48) | copy-start | bytes 786436
  83.8 21.2 %collective-permute-start.13 = (bf16[1536,256]{1,0:T(8,128)(2,1)S(1)}, bf16[1536,256]{1,0:T(8,128)(2,1)S(1)}, u32[]{:S(2)}, u32[]{:S(2)}) collective-permute-start(bf16[1536,256]{1,0:T(8,128)(2,1)S(1)} %slice.271), channel_id=1, source_target_pairs={{0,1},{1,0},{2,3},{3,2},{4,5},{5,4},{6,7},{7,6},{8,9},{9,8},{10,11... | collective-permute-start | bytes 2359304 | tf_op jit(solution)/shard_map/ppermute | solution.py:29
  86.8 15.0 %collective-permute-start.10 = (bf16[768,384]{1,0:T(8,128)(2,1)S(1)}, bf16[768,384]{1,0:T(8,128)(2,1)S(1)}, u32[]{:S(2)}, u32[]{:S(2)}) collective-permute-start(bf16[768,384]{1,0:T(8,128)(2,1)S(1)} %collective-permute-done.6), channel_id=1, source_target_pairs={{0,4},{4,0},{8,12},{12,8},{16,20},{20,16},{24,28},{28,24},{1,5},{5... | collective-permute-start | bytes 1769480 | tf_op jit(solution)/shard_map/ppermute | solution.py:293
  87.1 16.3 %collective-permute-start.7 = (bf16[768,384]{1,0:T(8,128)(2,1)S(1)}, bf16[768,384]{1,0:T(8,128)(2,1)S(1)}, u32[]{:S(2)}, u32[]{:S(2)}) collective-permute-start(bf16[768,384]{1,0:T(8,128)(2,1)S(1)} %collective-permute-done.6), channel_id=1, source_target_pairs={{0,8},{4,12},{8,16},{12,20},{16,24},{20,28},{24,0},{28,4},{1,9},{5... | collective-permute-start | bytes 1769480 | tf_op jit(solution)/shard_map/ppermute | solution.py:296
  102.1 17.4 %collective-permute-start.11 = (bf16[1536,256]{1,0:T(8,128)(2,1)S(1)}, bf16[1536,256]{1,0:T(8,128)(2,1)S(1)}, u32[]{:S(2)}, u32[]{:S(2)}) collective-permute-start(bf16[1536,256]{1,0:T(8,128)(2,1)S(1)} %slice.267), channel_id=1, source_target_pairs={{0,1},{1,0},{2,3},{3,2},{4,5},{5,4},{6,7},{7,6},{8,9},{9,8},{10,11... | collective-permute-start | bytes 2359304 | tf_op jit(solution)/shard_map/ppermute | solution.py:29
  103.4 15.9 %collective-permute-start.8 = (bf16[768,384]{1,0:T(8,128)(2,1)S(1)}, bf16[768,384]{1,0:T(8,128)(2,1)S(1)}, u32[]{:S(2)}, u32[]{:S(2)}) collective-permute-start(bf16[768,384]{1,0:T(8,128)(2,1)S(1)} %collective-permute-done.7), channel_id=1, source_target_pairs={{0,4},{4,0},{8,12},{12,8},{16,20},{20,16},{24,28},{28,24},{1,5},{5... | collective-permute-start | bytes 1769480 | tf_op jit(solution)/shard_map/ppermute | solution.py:293
  119.5 14.4 %collective-permute-start.9 = (bf16[1536,256]{1,0:T(8,128)(2,1)S(1)}, bf16[1536,256]{1,0:T(8,128)(2,1)S(1)}, u32[]{:S(2)}, u32[]{:S(2)}) collective-permute-start(bf16[1536,256]{1,0:T(8,128)(2,1)S(1)} %slice.238), channel_id=1, source_target_pairs={{0,1},{1,0},{2,3},{3,2},{4,5},{5,4},{6,7},{7,6},{8,9},{9,8},{10,11... | collective-permute-start | bytes 2359304 | tf_op jit(solution)/shard_map/ppermute | solution.py:29
  149.6 2.6 %collective-permute-start.17 = (bf16[192,2048]{1,0:T(8,128)(2,1)S(1)}, bf16[192,2048]{1,0:T(8,128)(2,1)}, u32[]{:S(2)}, u32[]{:S(2)}) collective-permute-start(bf16[192,2048]{1,0:T(8,128)(2,1)S(1)} %convolution_convert_fusion.4), channel_id=1, source_target_pairs={{0,1},{1,0},{2,3},{3,2},{4,5},{5,4},{6,7},{7,6},{8,9},{9,8},{10,11... | collective-permute-start | bytes 2359304 | tf_op jit(solution)/shard_map/ppermute | solution.py:29
  151.7 3.4 %collective-permute-start.16 = (bf16[192,2048]{1,0:T(8,128)(2,1)S(1)}, bf16[192,2048]{1,0:T(8,128)(2,1)S(1)}, u32[]{:S(2)}, u32[]{:S(2)}) collective-permute-start(bf16[192,2048]{1,0:T(8,128)(2,1)S(1)} %convolution_convert_fusion.6), channel_id=1, source_target_pairs={{0,1},{1,0},{2,3},{3,2},{4,5},{5,4},{6,7},{7,6},{8,9},{9,8},{10,11... | collective-permute-start | bytes 2359304 | tf_op jit(solution)/shard_map/ppermute | solution.py:29
  153.9 19.9 %collective-permute-start.18 = (bf16[192,2048]{1,0:T(8,128)(2,1)S(1)}, bf16[192,2048]{1,0:T(8,128)(2,1)S(1)}, u32[]{:S(2)}, u32[]{:S(2)}) collective-permute-start(bf16[192,2048]{1,0:T(8,128)(2,1)S(1)} %add_convert_fusion.1), channel_id=1, source_target_pairs={{0,2},{1,3},{2,0},{3,1},{4,6},{5,7},{6,4},{7,5},{8,10},{9,11},{10,... | collective-permute-start | bytes 2359304 | tf_op jit(solution)/shard_map/ppermute | solution.py:29
  154.5 20.5 %copy-start.1 = (bf16[768,384]{1,0:T(8,128)(2,1)S(1)}, bf16[768,384]{1,0:T(8,128)(2,1)}, u32[]{:S(2)}) copy-start(bf16[768,384]{1,0:T(8,128)(2,1)} %param.27) | copy-start | bytes 1769476
  (3 other events, 3.3 us)
